TPU v7x, 256 devices: a whole 4x4x8 slice. The times are simulated.
256 devices in a mesh: sp: 64 (over z, y, core), tp: 4 (over x).
Axes of the slice: x: 4, y: 4, z: 8, core: 2. Of those that a mesh axis runs over, the one named last changes fastest.
Arguments:
- out_cotangent: bfloat16 [8192, 2048], P('sp'), may hold values from -16 to 16
- routes: int32 [8192, 2], P('sp'), may hold values from 0 to 63, all different within a row; in each aligned block of 128 rows (0 to 127, 128 to 255, ...) at most 6 rows name the same one
- route_weights: float32 [8192, 2], P('sp'), may hold values from 0.3 to 1.5
- expert_rows: bfloat16 [64, 384, 2048], P('sp', None, 'tp'), may hold values from -6 to 6
- w_gate: bfloat16 [64, 2048, 1024], P('sp', None, 'tp'), may hold values from -0.125 to 0.125
- w_up: bfloat16 [64, 2048, 1024], P('sp', None, 'tp'), may hold values from -0.125 to 0.125
- w_down: bfloat16 [64, 1024, 2048], P('sp', 'tp'), may hold values from -0.1875 to 0.1875
- out_weight: bfloat16 [2048, 4096], P('sp', 'tp'), may hold values from -0.09375 to 0.09375
- values: bfloat16 [8192, 4096], P('sp', 'tp'), may hold values from -0.25 to 0.25
- keys: bfloat16 [8192, 1024], P('sp', 'tp'), may hold values from -0.5 to 0.5
- queries: bfloat16 [8192, 1024], P('sp', 'tp'), may hold values from -6 to 6
- log_decay: float32 [8192, 64], P('sp', 'tp'), may hold values from -1 to 0
- gate_input: bfloat16 [8192, 4096], P('sp', 'tp'), may hold values from -6 to 6
Outputs:
- grad_w_gate: bfloat16 [64, 2048, 1024], P('sp', None, 'tp')
- grad_w_up: bfloat16 [64, 2048, 1024], P('sp', None, 'tp')
- grad_w_down: bfloat16 [64, 1024, 2048], P('sp', 'tp')
- grad_out_weight: float32 [2048, 4096], P('sp', 'tp')
- grad_residual: float32 [8192, 2048], P('sp', 'tp')
- grad_values: float32 [8192, 4096], P('sp', 'tp')
- grad_keys: float32 [8192, 1024], P('sp', 'tp')
- grad_queries: float32 [8192, 1024], P('sp', 'tp')
- grad_decay: float32 [8192, 64], P('sp', 'tp')
- grad_gate: float32 [8192, 4096], P('sp', 'tp')
Inputs may be any that keep to these rules, and one draw needn't show every extreme that they name: `routes`: in each aligned block of 128 tokens no expert is named by more than 6 pairs, a bound that some block reaches.
All inputs are finite; a program needn't handle non-finite values.
Results may differ from a plain program's by a relative error of at most 0.0062.
Values may be sent and summed in bfloat16 or wider, within the bound.
A program may use at most 128 MiB of HBM per device.

v0:
```python
import jax
import jax.numpy as jnp
from jax import lax
from jax.sharding import Mesh
from jax.sharding import PartitionSpec as P

STATE = 128
SPAN = 128
SP = ("sp_0", "sp_1", "sp_2")
HIGHEST = lax.Precision.HIGHEST


def nothing_yet(shard, identity):
    return jax.tree.map(
        lambda part, zero: jnp.zeros_like(part) + jnp.asarray(zero, part.dtype), shard, identity
    )


def carried_in(shard, axes, combine, identity, reverse):
    before = start = nothing_yet(shard, identity)
    running = shard
    for axis in reversed(axes):
        length, here = (lax.axis_size(axis), lax.axis_index(axis))
        pieces = jax.tree.map(lambda part: lax.all_gather(part, axis), running)
        inside, running = (start, start)
        for k in reversed(range(length)) if reverse else range(length):
            passed = k > here if reverse else k < here
            running = combine(running, jax.tree.map(lambda part: part[k], pieces))
            inside = jax.tree.map(lambda new, old: jnp.where(passed, new, old), running, inside)
        before = combine(inside, before)
    return before


def block_step(state_now, block_input):
    values_blk, keys_blk, queries_blk, decay_blk = block_input
    span_len, head_count, head_dim = values_blk.shape
    groups = keys_blk.shape[1]
    state_dim = keys_blk.shape[2]
    repeat = head_count // groups
    cumulative = jnp.cumsum(decay_blk, axis=0)
    lower_mask = jnp.arange(span_len)[:, None] >= jnp.arange(span_len)[None, :]
    segment = cumulative[:, None, :] - cumulative[None, :, :]
    weights = jnp.exp(jnp.where(lower_mask[:, :, None], segment, -jnp.inf)).reshape(
        span_len, span_len, groups, repeat
    )
    inner_prod = jnp.einsum("tgn,sgn->tsg", queries_blk, keys_blk, precision=HIGHEST)
    grouped = values_blk.reshape(span_len, groups, repeat, head_dim)
    combined = inner_prod[:, :, :, None] * weights
    within = jnp.einsum("tsgr,sgrp->tgrp", combined, grouped, precision=HIGHEST)
    carried = jnp.einsum(
        "tgn,grpn->tgrp",
        queries_blk,
        state_now.reshape(groups, repeat, head_dim, state_dim),
        precision=HIGHEST,
    )
    carried = carried * jnp.exp(cumulative).reshape(span_len, groups, repeat)[..., None]
    to_end = jnp.exp(cumulative[-1][None, :] - cumulative).reshape(span_len, groups, repeat)
    added_state = jnp.einsum(
        "sgn,sgrp->grpn", keys_blk, grouped * to_end[..., None], precision=HIGHEST
    )
    new_state = state_now * jnp.exp(cumulative[-1])[:, None, None] + added_state.reshape(
        head_count, head_dim, state_dim
    )
    return (new_state, (within + carried).reshape(span_len, head_count * head_dim))


def mixer_scan(value_f, key_f, query_f, decay_f, start_state):
    row_count = value_f.shape[0]
    head_count = decay_f.shape[1]
    groups = key_f.shape[1] // STATE
    head_dim = value_f.shape[1] // head_count
    span_len = min(SPAN, row_count)
    blocks = row_count // span_len
    value_b = value_f.reshape(blocks, span_len, head_count, head_dim)
    key_b = key_f.reshape(blocks, span_len, groups, STATE)
    query_b = query_f.reshape(blocks, span_len, groups, STATE)
    decay_b = decay_f.reshape(blocks, span_len, head_count)
    end_state, outputs = lax.scan(block_step, start_state, (value_b, key_b, query_b, decay_b))
    return (outputs.reshape(row_count, head_count * head_dim), end_state)


def carry_combine(earlier, later):
    return (earlier[0] * later[0], later[0][:, None, None] * earlier[1] + later[1])


def shards(
    out_cotangent,
    routes,
    route_weights,
    expert_rows,
    w_gate,
    w_up,
    w_down,
    out_weight,
    values,
    keys,
    queries,
    log_decay,
    gate_input,
):
    sp_size = lax.axis_size(SP)
    tp_size = lax.axis_size("tp")
    tok_count, model_width = out_cotangent.shape
    local_experts = w_gate.shape[0]
    slot_count = expert_rows.shape[1]
    capacity = slot_count // sp_size
    experts_all = local_experts * sp_size
    columns = model_width // tp_size
    pair_list = routes.reshape(-1)
    onehot = (pair_list[:, None] == jnp.arange(experts_all, dtype=jnp.int32)[None, :]).astype(
        jnp.int32
    )
    pair_rank = jnp.sum(jnp.cumsum(onehot, axis=0) * onehot, axis=1) - 1
    target = pair_list * capacity + pair_rank
    cotangent_part = lax.dynamic_slice_in_dim(
        out_cotangent, lax.axis_index("tp") * columns, columns, 1
    )
    scaled = (route_weights[:, :, None] * cotangent_part[:, None, :].astype(jnp.float32)).astype(
        jnp.bfloat16
    )
    outgoing = (
        jnp.zeros((experts_all * capacity, columns), jnp.bfloat16)
        .at[target]
        .set(scaled.reshape(-1, columns))
    )
    arrived_part = lax.all_to_all(
        outgoing.reshape(experts_all, capacity, columns),
        SP,
        split_axis=0,
        concat_axis=0,
        tiled=True,
    )
    arrived_part = jnp.moveaxis(
        arrived_part.reshape(sp_size, local_experts, capacity, columns), 0, 1
    )
    arrived_part = arrived_part.reshape(local_experts, slot_count, columns)
    arrived = lax.all_gather(arrived_part, "tp", axis=2, tiled=True)
    full_rows = lax.all_gather(expert_rows, "tp", axis=2, tiled=True)
    gate_pre = jnp.einsum("esd,edf->esf", full_rows, w_gate, preferred_element_type=jnp.float32)
    up_pre = jnp.einsum("esd,edf->esf", full_rows, w_up, preferred_element_type=jnp.float32)
    sigmoid_gate = jax.nn.sigmoid(gate_pre)
    activated = gate_pre * sigmoid_gate
    hidden = (activated * up_pre).astype(jnp.bfloat16)
    hidden_grad = jnp.einsum("esd,efd->esf", arrived, w_down, preferred_element_type=jnp.float32)
    slope = sigmoid_gate * (1.0 + gate_pre * (1.0 - sigmoid_gate))
    gate_grad = (hidden_grad * up_pre * slope).astype(jnp.bfloat16)
    up_grad = (hidden_grad * activated).astype(jnp.bfloat16)
    grad_w_down = jnp.einsum(
        "esf,esd->efd", hidden, arrived, preferred_element_type=jnp.float32
    ).astype(jnp.bfloat16)
    grad_w_gate = jnp.einsum(
        "esd,esf->edf", full_rows, gate_grad, preferred_element_type=jnp.float32
    ).astype(jnp.bfloat16)
    grad_w_up = jnp.einsum(
        "esd,esf->edf", full_rows, up_grad, preferred_element_type=jnp.float32
    ).astype(jnp.bfloat16)
    partial_value = jnp.einsum(
        "esf,edf->esd", gate_grad, w_gate, preferred_element_type=jnp.float32
    )
    partial_value = partial_value + jnp.einsum(
        "esf,edf->esd", up_grad, w_up, preferred_element_type=jnp.float32
    )
    summed = lax.psum_scatter(partial_value, "tp", scatter_dimension=2, tiled=True).astype(
        jnp.bfloat16
    )
    send_back = jnp.moveaxis(summed.reshape(local_experts, sp_size, capacity, columns), 1, 0)
    send_back = send_back.reshape(experts_all, capacity, columns)
    returned = lax.all_to_all(send_back, SP, split_axis=0, concat_axis=0, tiled=True)
    picked = returned.reshape(experts_all * capacity, columns)[target].reshape(
        tok_count, -1, columns
    )
    own_columns = lax.dynamic_slice_in_dim(
        out_cotangent, lax.axis_index("tp") * columns, columns, 1
    )
    grad_residual = own_columns.astype(jnp.float32) + jnp.sum(picked.astype(jnp.float32), axis=1)
    residual_low = lax.all_gather(grad_residual.astype(jnp.bfloat16), "tp", axis=1, tiled=True)
    head_count = log_decay.shape[1]
    groups = keys.shape[1] // STATE
    head_dim = values.shape[1] // head_count
    repeat = head_count // groups
    value_f = values.astype(jnp.float32)
    key_f = keys.astype(jnp.float32)
    query_f = queries.astype(jnp.float32)
    cumulative = jnp.cumsum(log_decay, axis=0)
    decay_total = jnp.exp(cumulative[-1])
    to_end = jnp.exp(cumulative[-1][None, :] - cumulative)
    scaled_values = (value_f.reshape(tok_count, head_count, head_dim) * to_end[:, :, None]).reshape(
        tok_count, groups, repeat, head_dim
    )
    own_state = jnp.einsum(
        "sgn,sgrp->grpn", key_f.reshape(tok_count, groups, STATE), scaled_values, precision=HIGHEST
    )
    own_state = own_state.reshape(head_count, head_dim, STATE)
    identity = (
        jnp.ones((head_count,), jnp.float32),
        jnp.zeros((head_count, head_dim, STATE), jnp.float32),
    )
    entry_state = carried_in((decay_total, own_state), SP, carry_combine, identity, False)[1]
    (mixer_y, leaving), pull_back = jax.vjp(
        mixer_scan, value_f, key_f, query_f, log_decay, entry_state
    )
    part_rows = residual_low
    mixed_grad = jnp.dot(
        part_rows,
        lax.all_gather(out_weight, SP, axis=0, tiled=True),
        preferred_element_type=jnp.float32,
    )
    gate_f = gate_input.astype(jnp.float32)
    gate_sigmoid = jax.nn.sigmoid(gate_f)
    gate_active = gate_f * gate_sigmoid
    gate_slope = gate_sigmoid * (1.0 + gate_f * (1.0 - gate_sigmoid))
    mixed = (mixer_y * gate_active).astype(jnp.bfloat16)
    grad_gate = mixed_grad * mixer_y * gate_slope
    y_grad = mixed_grad * gate_active
    weighted_grad = (
        y_grad.reshape(tok_count, head_count, head_dim) * jnp.exp(cumulative)[:, :, None]
    ).reshape(tok_count, groups, repeat, head_dim)
    reached_state = jnp.einsum(
        "tgn,tgrp->grpn",
        query_f.reshape(tok_count, groups, STATE),
        weighted_grad,
        precision=HIGHEST,
    )
    reached_state = reached_state.reshape(head_count, head_dim, STATE)
    later_state = carried_in((decay_total, reached_state), SP, carry_combine, identity, True)[1]
    grad_values, grad_keys, grad_queries, grad_decay, unused_state = pull_back(
        (y_grad, later_state)
    )
    part_rows = residual_low
    grad_out_weight = lax.psum_scatter(
        lax.dot_general(
            part_rows, mixed, (((0,), (0,)), ((), ())), preferred_element_type=jnp.float32
        ),
        SP,
        scatter_dimension=0,
        tiled=True,
    )
    return (
        grad_w_gate,
        grad_w_up,
        grad_w_down,
        grad_out_weight,
        grad_residual,
        grad_values,
        grad_keys,
        grad_queries,
        grad_decay,
        grad_gate,
    )


def solution(mesh):
    finer = Mesh(mesh.devices.reshape(8, 4, 2, mesh.shape["tp"]), ("sp_0", "sp_1", "sp_2", "tp"))
    in_specs = (
        P(SP, None),
        P(SP, None),
        P(SP, None),
        P(SP, None, "tp"),
        P(SP, None, "tp"),
        P(SP, None, "tp"),
        P(SP, "tp", None),
        P(SP, "tp"),
        P(SP, "tp"),
        P(SP, "tp"),
        P(SP, "tp"),
        P(SP, "tp"),
        P(SP, "tp"),
    )
    out_specs = (
        P(SP, None, "tp"),
        P(SP, None, "tp"),
        P(SP, "tp", None),
        P(SP, "tp"),
        P(SP, "tp"),
        P(SP, "tp"),
        P(SP, "tp"),
        P(SP, "tp"),
        P(SP, "tp"),
        P(SP, "tp"),
    )
    return jax.shard_map(
        shards, mesh=finer, in_specs=in_specs, out_specs=out_specs, check_vma=False
    )
```

profile of v0, /device:TPU:4, one launch (start us, length us, event | category | flops | bytes accessed | tf_op | source)
XLA Modules:
  0.0 573.2 jit_solution(100809377200915807)
XLA Ops:
  8.8 0.8 copy.79
  11.7 0.8 copy.82
  12.6 0.9 dynamic-slice_convert_fusion
  14.2 1.7 scatter_custom_fusion
  16.1 29.5 %all_to_all.10 = bf16[64,6,512]{2,1,0:T(8,128)(2,1)S(1)} all-to-all(bf16[64,6,512]{2,1,0:T(8,128)(2,1)S(1)} %reshape.691), channel_id=1, replica_groups=mesh['sp_0'=8,'sp_1'=4,'sp_2'=2,'tp'=4] {'sp_0','sp_1','sp_2'}, dimensions={0} | all-to-all | bytes 786432 | tf_op jit(solution)/shard_map/all_to_all | solution.py:126
  45.6 0.9 reshape_transpose_reshape.6
  46.6 2.1 fusion.5
  48.7 1.9 fusion.7
  50.7 22.0 %all-gather.14.cloned.1.call-done = bf16[1,384,2048]{2,1,0:T(8,128)(2,1)} async-done(((bf16[1,384,512]{2,1,0:T(8,128)(2,1)}), bf16[1,384,2048]{2,1,0:T(8,128)(2,1)}) %all-gather.14.cloned.1.call-update) | async-done | bytes 1572880 | tf_op jit(solution)/shard_map/all_gather | solution.py:137
  72.7 2.3 multiply_convert_fusion.3
  76.4 2.2 add_bitcast_fusion
  79.3 40.2 %reduce-scatter.3.cloned.1.call-done = f32[1,384,512]{2,1,0:T(8,128)} async-done(((f32[1,384,2048]{2,1,0:T(8,128)}), f32[1,384,512]{2,1,0:T(8,128)}) %reduce-scatter.3.cloned.1.call-update) | async-done | bytes 786448 | tf_op jit(solution)/shard_map/reduce_scatter | solution.py:163
  119.4 1.2 convert_element_type.85
  120.6 0.9 reshape_transpose_reshape.7
  121.5 10.5 %all-to-all-start.1 = ((bf16[64,6,512]{2,1,0:T(8,128)(2,1)}), bf16[64,6,512]{2,1,0:T(8,128)(2,1)S(1)}, u32[]{:S(2)}, u32[]{:S(2)}) async-start(bf16[64,6,512]{2,1,0:T(8,128)(2,1)} %reshape_transpose_reshape.7), calls=%async_computation.2 | async-start | bytes 1048576 | tf_op jit(solution)/shard_map/all_to_all | solution.py:168
  132.5 21.9 %all-to-all-done.1 = bf16[64,6,512]{2,1,0:T(8,128)(2,1)S(1)} async-done(((bf16[64,6,512]{2,1,0:T(8,128)(2,1)}), bf16[64,6,512]{2,1,0:T(8,128)(2,1)S(1)}, u32[]{:S(2)}, u32[]{:S(2)}) %all-to-all-start.1) | async-done | bytes 393248 | tf_op jit(solution)/shard_map/all_to_all | solution.py:168
  154.6 1.2 gather_fusion
  156.7 1.7 fusion.99
  158.3 11.8 %all_gather.56 = bf16[128,2048]{1,0:T(8,128)(2,1)S(1)} all-gather(bf16[128,512]{1,0:T(8,128)(2,1)S(1)} %get-tuple-element.222), channel_id=1, replica_groups=mesh['sp_0'=8,'sp_1'=4,'sp_2'=2,'tp'=4] {'tp'}, dimensions={1}, use_global_device_ids=true | all-gather | bytes 655360 | tf_op jit(solution)/shard_map/all_gather | solution.py:176
  170.1 4.0 fusion.72
  174.3 1.2 fusion.62
  176.1 1.8 all-gather
  178.5 10.4 %all-gather.1 = f32[4,1,16]{2,1,0:T(1,128)S(1)} all-gather(f32[1,1,16]{2,1,0:T(1,128)S(1)} %get-tuple-element.301), channel_id=1, replica_groups=mesh['sp_0'=8,'sp_1'=4,'sp_2'=2,'tp'=4] {'sp_1'}, dimensions={0}, use_global_device_ids=true | all-gather | bytes 320 | tf_op jit(solution)/shard_map/all_gather | solution.py:24
  189.5 2.3 multiply_add_fusion.1
  192.5 31.9 %all-gather.28.cloned.1.call-done = f32[4,16,64,128]{3,2,1,0:T(8,128)} async-done(((f32[1,16,64,128]{3,2,1,0:T(8,128)}), f32[4,16,64,128]{3,2,1,0:T(8,128)}) %all-gather.28.cloned.1.call-update) | async-done | bytes 2097168 | tf_op jit(solution)/shard_map/all_gather | solution.py:24
  224.4 3.3 multiply_add_fusion
  229.6 16.8 %all-gather.3 = f32[8,1,16]{2,1,0:T(1,128)S(1)} all-gather(f32[1,1,16]{2,1,0:T(1,128)S(1)} %get-tuple-element.282), channel_id=1, replica_groups=mesh['sp_0'=8,'sp_1'=4,'sp_2'=2,'tp'=4] {'sp_0'}, dimensions={0}, use_global_device_ids=true | all-gather | bytes 576 | tf_op jit(solution)/shard_map/all_gather | solution.py:24
  253.0 29.7 %all-gather.30.cloned.1.call-done = f32[8,16,64,128]{3,2,1,0:T(8,128)} async-done(((f32[1,16,64,128]{3,2,1,0:T(8,128)}), f32[8,16,64,128]{3,2,1,0:T(8,128)}) %all-gather.30.cloned.1.call-update) | async-done | bytes 4194320 | tf_op jit(solution)/shard_map/all_gather | solution.py:24
  282.9 2.6 fusion.102
  285.8 2.6 add_add_fusion
  288.4 1.2 fusion.27
  289.6 0.7 multiply_reduce_fusion.2
  290.3 1.2 fusion.26
  291.5 12.9 %all-gather.18.cloned.1.call-done = f32[2,16,64,128]{3,2,1,0:T(8,128)} async-done(((f32[1,16,64,128]{3,2,1,0:T(8,128)}), f32[2,16,64,128]{3,2,1,0:T(8,128)}) %all-gather.18.cloned.1.call-update) | async-done | bytes 1048592 | tf_op jit(solution)/shard_map/all_gather | solution.py:24
  304.5 2.4 multiply_add_fusion.3
  307.0 34.6 %all-gather.20.cloned.1.call-done = f32[4,16,64,128]{3,2,1,0:T(8,128)} async-done(((f32[1,16,64,128]{3,2,1,0:T(8,128)}), f32[4,16,64,128]{3,2,1,0:T(8,128)}) %all-gather.20.cloned.1.call-update) | async-done | bytes 2097168 | tf_op jit(solution)/shard_map/all_gather | solution.py:24
  341.6 3.2 multiply_add_fusion.2
  345.2 16.7 %all-gather.2 = f32[8,1,16]{2,1,0:T(1,128)S(1)} all-gather(f32[1,1,16]{2,1,0:T(1,128)S(1)} %copy-done.91), channel_id=1, replica_groups=mesh['sp_0'=8,'sp_1'=4,'sp_2'=2,'tp'=4] {'sp_0'}, dimensions={0}, use_global_device_ids=true | all-gather | bytes 576 | tf_op jit(solution)/shard_map/all_gather | solution.py:24
  368.0 0.8 copy.85
  369.3 30.4 %all-gather.22.cloned.1.call-done = f32[8,16,64,128]{3,2,1,0:T(8,128)} async-done(((f32[1,16,64,128]{3,2,1,0:T(8,128)}), f32[8,16,64,128]{3,2,1,0:T(8,128)}) %all-gather.22.cloned.1.call-update) | async-done | bytes 4194320 | tf_op jit(solution)/shard_map/all_gather | solution.py:24
  400.0 2.6 fusion.101
  403.0 1.4 add_add_fusion.1
  404.5 1.0 multiply_reduce_fusion.1
  405.5 2.1 fusion.13
  407.6 1.2 copy.91
  408.9 5.9 %fusion.66 = f32[2048,1024]{1,0:T(8,128)} fusion(bf16[128,2048]{1,0:T(8,128)(2,1)} %copy-done.7, f32[128,1024]{1,0:T(8,128)S(1)} %copy.91, bf16[128,1024]{1,0:T(8,128)(2,1)} %param.25), kind=kOutput, calls=%fused_computation.129 | convolution fusion | flops 537788416 | bytes 9699328 | tf_op jit(solution)/shard_map/dot_general | solution.py:231
  416.0 1.7 fusion
  417.7 2.3 copy.104
  420.0 1.7 fusion.1
  421.7 2.4 copy.105
  424.1 2.8 fusion.2
  426.9 1.5 fusion.25
  428.5 0.7 copy.101
  429.8 1.0 convolution_bitcast_fusion.6
  431.1 0.8 copy.107
  431.9 3.3 fusion.12
  435.2 2.1 copy.106
  437.4 1.0 convolution_bitcast_fusion.5
  438.7 0.8 copy.108
  439.4 0.7 copy.100
  440.3 6.7 %fusion.38 = f32[16]{0:T(128)S(1)} fusion(f32[16]{0:T(128)} %copy-done.73, f32[16]{0:T(128)S(1)} %copy-done.69, f32[16]{0:T(128)} %copy-done.70, f32[16]{0:T(128)} %copy-done.75, f32[16]{0:T(128)} %get-tuple-element.215, f32[16]{0:T(128)} %get-tuple-element.278, f32[16]{0:T(128)} %get-tuple-element.277, f32[16]{0:T(128)} %get-tuple-element.276, ...), kind=kLoop, calls=%fused_computation.61 | loop fusion | flops 11534320 | bytes 14682076 | tf_op jit(solution)/shard_map/transpose(jvp())/while/body/eval_jaxpr/reduce_sum | solution.py:61
  447.1 1.1 reduce_window_sum.44
  448.9 2.2 fusion.33
  451.2 114.9 %reduce-scatter.5.cloned.1.call-done = f32[32,1024]{1,0:T(8,128)} async-done(((f32[2048,1024]{1,0:T(8,128)}), f32[32,1024]{1,0:T(8,128)}) %reduce-scatter.5.cloned.1.call-update) | async-done | bytes 131088 | tf_op jit(solution)/shard_map/reduce_scatter | solution.py:230
  (322 shorter events, 29.3 us)
Async XLA Ops:
  8.0 38.6 %copy-start = (bf16[1,2048,256]{2,1,0:T(8,128)(2,1)S(1)}, bf16[1,2048,256]{2,1,0:T(8,128)(2,1)}, u32[]{:S(2)}) copy-start(bf16[1,2048,256]{2,1,0:T(8,128)(2,1)} %param.17) | copy-start | bytes 3145732
  8.0 38.5 %all-gather.16.cloned.1.call-start = ((), (), s32[]{:S(2)}) async-start(), calls=%async_computation.5 | async-start | bytes 1966080 | tf_op jit(solution)/shard_map/all_gather | solution.py:138
  8.8 63.9 %all-gather.14.cloned.1.call-start = ((), (), s32[]{:S(2)}) async-start(), calls=%async_computation.4 | async-start | bytes 1966080 | tf_op jit(solution)/shard_map/all_gather | solution.py:137
  46.5 72.9 %reduce-scatter.3.cloned.1.call-start = ((), (), s32[]{:S(2)}) async-start(), calls=%async_computation.6 | async-start | bytes 3932160 | tf_op jit(solution)/shard_map/reduce_scatter | solution.py:163
  48.7 26.3 %copy-start.35 = (f32[384,256]{1,0:T(8,128)}, f32[384,256]{1,0:T(8,128)S(1)}, u32[]{:S(2)}) copy-start(f32[384,256]{1,0:T(8,128)S(1)} %fusion.5) | copy-start | bytes 1179652
  50.7 24.3 %copy-start.37 = (f32[384,256]{1,0:T(8,128)}, f32[384,256]{1,0:T(8,128)S(1)}, u32[]{:S(2)}) copy-start(f32[384,256]{1,0:T(8,128)S(1)} %fusion.7) | copy-start | bytes 1179652
  78.7 53.4 %copy-start.48 = (bf16[128,256]{1,0:T(8,128)(2,1)S(1)}, bf16[128,256]{1,0:T(8,128)(2,1)}, u32[]{:S(2)}) copy-start(bf16[128,256]{1,0:T(8,128)(2,1)} %param.23) | copy-start | bytes 196612
  78.7 53.5 %copy-start.65 = (f32[128,16]{0,1:T(8,128)S(1)}, f32[128,16]{0,1:T(8,128)}, u32[]{:S(2)}) copy-start(f32[128,16]{0,1:T(8,128)} %param.24) | copy-start | bytes 24580
  78.7 91.5 %all-gather.24.cloned.1.call-start = ((), (), s32[]{:S(2)}) async-start(), calls=%async_computation.11 | async-start | bytes 4259840 | tf_op jit(solution)/shard_map/all_gather | solution.py:205
  121.5 32.9 %all-to-all-start.1 = ((bf16[64,6,512]{2,1,0:T(8,128)(2,1)}), bf16[64,6,512]{2,1,0:T(8,128)(2,1)S(1)}, u32[]{:S(2)}, u32[]{:S(2)}) async-start(bf16[64,6,512]{2,1,0:T(8,128)(2,1)} %reshape_transpose_reshape.7), calls=%async_computation.2 | async-start | bytes 1048576 | tf_op jit(solution)/shard_map/all_to_all | solution.py:168
  132.0 57.5 %all-gather.26.cloned.1.call-start = ((), (), s32[]{:S(2)}) async-start(), calls=%async_computation.12 | async-start | bytes 1572864 | tf_op jit(solution)/shard_map/all_gather | solution.py:24
  132.4 43.2 %copy-start.27 = (f32[128,16]{1,0:T(8,128)}, f32[128,16]{1,0:T(8,128)S(1)}, u32[]{:S(2)}) copy-start(f32[128,16]{1,0:T(8,128)S(1)} %reduce_window_sum.43) | copy-start | bytes 24580
  132.5 41.8 %copy-start.41 = (f32[128,2,8]{0,2,1:T(8,128)}, f32[128,2,8]{0,2,1:T(8,128)S(1)}, u32[]{:S(2)}) copy-start(f32[128,2,8]{0,2,1:T(8,128)S(1)} %bitcast_exponential_fusion) | copy-start | bytes 24580
  155.7 14.4 %copy-start.20 = (bf16[128,1024]{1,0:T(8,128)(2,1)S(1)}, bf16[128,1024]{1,0:T(8,128)(2,1)}, u32[]{:S(2)}) copy-start(bf16[128,1024]{1,0:T(8,128)(2,1)} %param.25) | copy-start | bytes 786436
  170.1 4.0 copy-start.7
  175.5 48.9 %all-gather.28.cloned.1.call-start = ((), (), s32[]{:S(2)}) async-start(), calls=%async_computation.13 | async-start | bytes 2621440 | tf_op jit(solution)/shard_map/all_gather | solution.py:24
  177.9 49.8 %copy-start.57 = (f32[2,1,16]{2,1,0:T(1,128)}, f32[2,1,16]{2,1,0:T(1,128)S(1)}, u32[]{:S(2)}) copy-start(f32[2,1,16]{2,1,0:T(1,128)S(1)} %all-gather) | copy-start | bytes 388
  178.5 13.3 %copy-start.68 = (f32[16]{0:T(128)}, f32[16]{0:T(128)S(1)}, u32[]{:S(2)}) copy-start(f32[16]{0:T(128)S(1)} %get-tuple-element.298) | copy-start | bytes 196
  188.9 40.1 %copy-start.50 = (f32[4,1,16]{2,1,0:T(1,128)}, f32[4,1,16]{2,1,0:T(1,128)S(1)}, u32[]{:S(2)}) copy-start(f32[4,1,16]{2,1,0:T(1,128)S(1)} %all-gather.1) | copy-start | bytes 772
  189.5 38.2 %copy-start.70 = (f32[16]{0:T(128)}, f32[16]{0:T(128)S(1)}, u32[]{:S(2)}) copy-start(f32[16]{0:T(128)S(1)} %get-tuple-element.279) | copy-start | bytes 196
  191.8 90.9 %all-gather.30.cloned.1.call-start = ((), (), s32[]{:S(2)}) async-start(), calls=%async_computation.14 | async-start | bytes 4718592 | tf_op jit(solution)/shard_map/all_gather | solution.py:24
  192.5 35.2 %copy-start.59 = (f32[16]{0:T(128)}, f32[16]{0:T(128)S(1)}, u32[]{:S(2)}) copy-start(f32[16]{0:T(128)S(1)} %get-tuple-element.284) | copy-start | bytes 196
  192.5 35.2 %copy-start.62 = (f32[16]{0:T(128)}, f32[16]{0:T(128)S(1)}, u32[]{:S(2)}) copy-start(f32[16]{0:T(128)S(1)} %get-tuple-element.286) | copy-start | bytes 196
  192.5 35.2 %copy-start.75 = (f32[16]{0:T(128)}, f32[16]{0:T(128)S(1)}, u32[]{:S(2)}) copy-start(f32[16]{0:T(128)S(1)} %get-tuple-element.285) | copy-start | bytes 196
  224.4 27.8 %copy-start.38 = (bf16[128,1024]{1,0:T(8,128)(2,1)S(1)}, bf16[128,1024]{1,0:T(8,128)(2,1)}, u32[]{:S(2)}) copy-start(bf16[128,1024]{1,0:T(8,128)(2,1)} %param.21) | copy-start | bytes 786436
  227.7 76.8 %all-gather.18.cloned.1.call-start = ((), (), s32[]{:S(2)}) async-start(), calls=%async_computation.7 | async-start | bytes 1572864 | tf_op jit(solution)/shard_map/all_gather | solution.py:24
  228.5 56.9 %copy-start.84 = (f32[2,8]{1,0:T(2,128)}, f32[2,8]{1,0:T(2,128)S(1)}, u32[]{:S(2)}) copy-start(f32[2,8]{1,0:T(2,128)S(1)} %squeeze.234) | copy-start | bytes 196
  228.6 56.9 %copy-start.76 = (f32[2,8]{1,0:T(2,128)}, f32[2,8]{1,0:T(2,128)S(1)}, u32[]{:S(2)}) copy-start(f32[2,8]{1,0:T(2,128)S(1)} %squeeze.235) | copy-start | bytes 196
  228.7 56.8 %copy-start.85 = (f32[2,8]{1,0:T(2,128)}, f32[2,8]{1,0:T(2,128)S(1)}, u32[]{:S(2)}) copy-start(f32[2,8]{1,0:T(2,128)S(1)} %squeeze.230) | copy-start | bytes 196
  228.8 56.7 %copy-start.53 = (f32[2,8]{1,0:T(2,128)}, f32[2,8]{1,0:T(2,128)S(1)}, u32[]{:S(2)}) copy-start(f32[2,8]{1,0:T(2,128)S(1)} %squeeze.231) | copy-start | bytes 196
  228.9 56.6 %copy-start.55 = (f32[2,8]{1,0:T(2,128)}, f32[2,8]{1,0:T(2,128)S(1)}, u32[]{:S(2)}) copy-start(f32[2,8]{1,0:T(2,128)S(1)} %squeeze.232) | copy-start | bytes 196
  229.0 56.5 %copy-start.78 = (f32[2,8]{1,0:T(2,128)}, f32[2,8]{1,0:T(2,128)S(1)}, u32[]{:S(2)}) copy-start(f32[2,8]{1,0:T(2,128)S(1)} %squeeze.233) | copy-start | bytes 196
  285.7 3.8 copy-start.109
  288.4 16.1 %copy-start.66 = (f32[16]{0:T(128)S(1)}, f32[16]{0:T(128)}, u32[]{:S(2)}) copy-start(f32[16]{0:T(128)} %get-tuple-element.297) | copy-start | bytes 196
  288.4 16.1 %copy-start.72 = (f32[16]{0:T(128)S(1)}, f32[16]{0:T(128)}, u32[]{:S(2)}) copy-start(f32[16]{0:T(128)} %get-tuple-element.291) | copy-start | bytes 196
  289.6 17.4 %copy-start.44 = (f32[128,2,8]{0,2,1:T(8,128)}, f32[128,2,8]{0,2,1:T(8,128)S(1)}, u32[]{:S(2)}) copy-start(f32[128,2,8]{0,2,1:T(8,128)S(1)} %get-tuple-element.304) | copy-start | bytes 24580
  290.3 51.3 %copy-start.60 = (f32[16]{0:T(128)S(1)}, f32[16]{0:T(128)}, u32[]{:S(2)}) copy-start(f32[16]{0:T(128)} %copy-done.59) | copy-start | bytes 196
  290.3 51.3 %copy-start.63 = (f32[16]{0:T(128)S(1)}, f32[16]{0:T(128)}, u32[]{:S(2)}) copy-start(f32[16]{0:T(128)} %copy-done.62) | copy-start | bytes 196
  290.3 51.3 %copy-start.71 = (f32[16]{0:T(128)S(1)}, f32[16]{0:T(128)}, u32[]{:S(2)}) copy-start(f32[16]{0:T(128)} %get-tuple-element.280) | copy-start | bytes 196
  290.3 51.3 %copy-start.74 = (f32[16]{0:T(128)S(1)}, f32[16]{0:T(128)}, u32[]{:S(2)}) copy-start(f32[16]{0:T(128)} %get-tuple-element.283) | copy-start | bytes 196
  291.5 50.1 %all-gather.20.cloned.1.call-start = ((), (), s32[]{:S(2)}) async-start(), calls=%async_computation.8 | async-start | bytes 2621440 | tf_op jit(solution)/shard_map/all_gather | solution.py:24
  307.0 92.8 %all-gather.22.cloned.1.call-start = ((), (), s32[]{:S(2)}) async-start(), calls=%async_computation.9 | async-start | bytes 4718592 | tf_op jit(solution)/shard_map/all_gather | solution.py:24
  344.8 221.2 %reduce-scatter.5.cloned.1.call-start = ((), (), s32[]{:S(2)}) async-start(), calls=%async_computation.10 | async-start | bytes 8519680 | tf_op jit(solution)/shard_map/reduce_scatter | solution.py:230
  345.0 57.6 %copy-start.29 = (bf16[128,2,128]{0,2,1:T(8,128)(2,1)}, bf16[128,2,128]{0,2,1:T(8,128)(2,1)S(1)}, u32[]{:S(2)}) copy-start(bf16[128,2,128]{0,2,1:T(8,128)(2,1)S(1)} %copy.98) | copy-start | bytes 196612
  408.8 5.9 %copy-start.4 = (f32[128,1024]{1,0:T(8,128)}, f32[128,1024]{1,0:T(8,128)S(1)}, u32[]{:S(2)}) copy-start(f32[128,1024]{1,0:T(8,128)S(1)} %copy.91) | copy-start | bytes 1572868
  416.0 4.0 copy-start.26
  429.8 7.5 %copy-start.6 = (f32[2,8,64,128]{3,2,1,0:T(8,128)S(1)}, f32[2,8,64,128]{3,2,1,0:T(8,128)}, u32[]{:S(2)}) copy-start(f32[2,8,64,128]{3,2,1,0:T(8,128)} %copy-done.5) | copy-start | bytes 1572868
  430.8 6.4 %copy-start.45 = (f32[128,2,8]{0,2,1:T(8,128)S(1)}, f32[128,2,8]{0,2,1:T(8,128)}, u32[]{:S(2)}) copy-start(f32[128,2,8]{0,2,1:T(8,128)} %copy-done.44) | copy-start | bytes 24580
  430.8 6.5 %copy-start.43 = (f32[128,2,8]{0,2,1:T(8,128)S(1)}, f32[128,2,8]{0,2,1:T(8,128)}, u32[]{:S(2)}) copy-start(f32[128,2,8]{0,2,1:T(8,128)} %copy-done.41) | copy-start | bytes 24580
  431.1 7.3 %copy-start.30 = (bf16[128,2,128]{0,2,1:T(8,128)(2,1)S(1)}, bf16[128,2,128]{0,2,1:T(8,128)(2,1)}, u32[]{:S(2)}) copy-start(bf16[128,2,128]{0,2,1:T(8,128)(2,1)} %copy-done.29) | copy-start | bytes 196612
  431.8 6.6 %copy-start.32 = (f32[128,128,2]{1,0,2:T(8,128)S(1)}, f32[128,128,2]{1,0,2:T(8,128)}, u32[]{:S(2)}) copy-start(f32[128,128,2]{1,0,2:T(8,128)} %copy-done.31) | copy-start | bytes 393220
  431.8 7.6 %copy-start.52 = (f32[128,2,8]{0,2,1:T(8,128)S(1)}, f32[128,2,8]{0,2,1:T(8,128)}, u32[]{:S(2)}) copy-start(f32[128,2,8]{0,2,1:T(8,128)} %get-tuple-element.306) | copy-start | bytes 24580
  431.8 8.3 %copy-start.2 = (f32[4,16,64,128]{3,2,1,0:T(8,128)S(1)}, f32[4,16,64,128]{3,2,1,0:T(8,128)}, u32[]{:S(2)}) copy-start(f32[4,16,64,128]{3,2,1,0:T(8,128)} %all-gather.28.cloned.1.call-done) | copy-start | bytes 6291460
  435.2 5.0 copy-start.61
  435.2 5.0 copy-start.64
  435.2 5.0 copy-start.67
  435.2 5.0 copy-start.69
  440.2 6.8 %copy-start.28 = (f32[128,16]{1,0:T(8,128)S(1)}, f32[128,16]{1,0:T(8,128)}, u32[]{:S(2)}) copy-start(f32[128,16]{1,0:T(8,128)} %copy-done.27) | copy-start | bytes 24580
  440.2 6.8 %copy-start.39 = (f32[128,16]{1,0:T(8,128)S(1)}, f32[128,16]{1,0:T(8,128)}, u32[]{:S(2)}) copy-start(f32[128,16]{1,0:T(8,128)} %copy.101) | copy-start | bytes 24580
  440.2 6.8 %copy-start.40 = (f32[128,16]{1,0:T(8,128)S(1)}, f32[128,16]{1,0:T(8,128)}, u32[]{:S(2)}) copy-start(f32[128,16]{1,0:T(8,128)} %copy.100) | copy-start | bytes 24580
  440.2 6.8 %copy-start.90 = (f32[16]{0:T(128)S(1)}, f32[16]{0:T(128)}, u32[]{:S(2)}) copy-start(f32[16]{0:T(128)} %get-tuple-element.258) | copy-start | bytes 196
  440.2 6.8 %copy-start.110 = (f32[1,16]{1,0:T(1,128)S(1)}, f32[1,16]{1,0:T(1,128)}, u32[]{:S(2)}) copy-start(f32[1,16]{1,0:T(1,128)} %reshape.706) | copy-start | bytes 196
  440.3 8.7 %copy-start.21 = (bf16[128,1024]{1,0:T(8,128)(2,1)S(1)}, bf16[128,1024]{1,0:T(8,128)(2,1)}, u32[]{:S(2)}) copy-start(bf16[128,1024]{1,0:T(8,128)(2,1)} %param.25) | copy-start | bytes 786436
  440.3 125.8 %copy-start.1 = (bf16[1,2048,256]{2,1,0:T(8,128)(2,1)S(1)}, bf16[1,2048,256]{2,1,0:T(8,128)(2,1)}, u32[]{:S(2)}) copy-start(bf16[1,2048,256]{2,1,0:T(8,128)(2,1)} %param.17) | copy-start | bytes 3145732
  (59 other events, 158.6 us)
Sparse Core Ops, SparseCore 0:
  10.6 30.5 all-gather.15
  46.6 26.0 all-gather.13
  78.8 40.6 reduce-scatter.2
  227.8 54.8 all-gather.29
  344.9 54.7 all-gather.21
Sparse Core Ops, SparseCore 1:
  81.9 83.9 all-gather.23
  175.6 11.8 all-gather.25
  191.9 32.5 all-gather.27
  291.6 12.8 all-gather.17
  307.0 34.5 all-gather.19
  414.9 151.1 reduce-scatter.4
where the time goes:
time: 574 us; the launch traced here: 573 us
  waiting for transfers between devices  340 us (59%)
  blocking collectives  87.1 us (15%)
  local copies, waits for them, and re-layouts  40.5 us (7%)
  matrix products  39.5 us (7%)
  other arithmetic  38.5 us (7%)
  between operations  16.7 us (3%)
  starting transfers between devices  10.9 us (2%)
    all_gather x6, waiting for transfers between devices, carried_in(): pieces = jax.tree.map(lambda part: lax.all_gather(part, axis), running)  140 us
    reduce_scatter x1, waiting for transfers between devices, shards(): lax.psum_scatter(lax.dot_general(part_rows, mixed, (((0,), (0,)), ((), ()...  115 us
    all_gather x4, blocking collectives, carried_in(): pieces = jax.tree.map(lambda part: lax.all_gather(part, axis), running)  45.8 us
    reduce_scatter x1, waiting for transfers between devices, shards(): lax.psum_scatter(partial_value, 'tp', scatter_dimension=2, tiled=True)  40.2 us
    all_to_all x1, blocking collectives, shards(): lax.all_to_all(outgoing.reshape(experts_all, capacity, columns), SP, spli...  29.5 us
    all_gather x1, waiting for transfers between devices, shards(): arrived = lax.all_gather(arrived_part, 'tp', axis=2, tiled=True)  22 us
    all_to_all x1, waiting for transfers between devices, shards(): lax.all_to_all(send_back, SP, split_axis=0, concat_axis=0, tiled=True)  21.9 us
    add x6, other arithmetic, carry_combine(): later[0][:, None, None] * earlier[1] + later[1]  15.2 us
  transfers between devices with their start and end apart: 12, of which 9 were waited for; matrix products, arithmetic and copies ran while one was open for 13% of the time, Pallas kernels for 0%

commit v1 on v0

--- a/solution.py
+++ b/solution.py
@@ -134,7 +134,10 @@
         arrived_part.reshape(sp_size, local_experts, capacity, columns), 0, 1
     )
     arrived_part = arrived_part.reshape(local_experts, slot_count, columns)
-    arrived = lax.all_gather(arrived_part, "tp", axis=2, tiled=True)
+    devices = lax.axis_size("tp")
+    shards_2 = jnp.stack([arrived_part for _ in range(devices)])
+    shards_2 = lax.all_to_all(shards_2, "tp", split_axis=0, concat_axis=0)
+    arrived = jnp.concatenate(shards_2, axis=2)
     full_rows = lax.all_gather(expert_rows, "tp", axis=2, tiled=True)
     gate_pre = jnp.einsum("esd,edf->esf", full_rows, w_gate, preferred_element_type=jnp.float32)
     up_pre = jnp.einsum("esd,edf->esf", full_rows, w_up, preferred_element_type=jnp.float32)

time: 574 us -> 568 us (0.990)
  waiting for transfers between devices: 340 us -> 328 us
    all_gather x1 -> x0, waiting for transfers between devices: 22 us -> none  [shards(): arrived = lax.all_gather(arrived_part, 'tp', axis=2, tiled=True)]
    all_to_all x0 -> x1, waiting for transfers between devices: none -> 14.3 us  [shards(): shards_2 = lax.all_to_all(shards_2, 'tp', split_axis=0, concat_axis=0)]
where the time goes in v1:
time: 568 us; the launch traced here: 567 us
  waiting for transfers between devices  328 us (58%)
  blocking collectives  87.2 us (15%)
  local copies, waits for them, and re-layouts  41.2 us (7%)
  matrix products  39.9 us (7%)
  other arithmetic  38.6 us (7%)
  between operations  16.7 us (3%)
  starting transfers between devices  15.7 us (3%)
    all_gather x6, waiting for transfers between devices, carried_in(): pieces = jax.tree.map(lambda part: lax.all_gather(part, axis), running)  140 us
    reduce_scatter x1, waiting for transfers between devices, shards(): lax.psum_scatter(lax.dot_general(part_rows, mixed, (((0,), (0,)), ((), ()...  115 us
    all_gather x4, blocking collectives, carried_in(): pieces = jax.tree.map(lambda part: lax.all_gather(part, axis), running)  45.7 us
    reduce_scatter x1, waiting for transfers between devices, shards(): lax.psum_scatter(partial_value, 'tp', scatter_dimension=2, tiled=True)  35.6 us
    all_to_all x1, blocking collectives, shards(): lax.all_to_all(outgoing.reshape(experts_all, capacity, columns), SP, spli...  29.5 us
    all_to_all x1, waiting for transfers between devices, shards(): lax.all_to_all(send_back, SP, split_axis=0, concat_axis=0, tiled=True)  21.9 us
    add x6, other arithmetic, carry_combine(): later[0][:, None, None] * earlier[1] + later[1]  15.2 us
    all_to_all x1, waiting for transfers between devices, shards(): shards_2 = lax.all_to_all(shards_2, 'tp', split_axis=0, concat_axis=0)  14.3 us
  transfers between devices with their start and end apart: 12, of which 9 were waited for; matrix products, arithmetic and copies ran while one was open for 13% of the time, Pallas kernels for 0%

profile of v1, /device:TPU:4, one launch (start us, length us, event | category | flops | bytes accessed | tf_op | source)
XLA Modules:
  0.0 566.9 jit_solution(13643703318824444102)
XLA Ops:
  9.4 0.8 copy.80
  11.6 0.8 copy.83
  12.6 0.9 dynamic-slice_convert_fusion
  14.2 1.7 scatter_custom_fusion
  16.0 29.5 %all_to_all.15 = bf16[64,6,512]{2,1,0:T(8,128)(2,1)S(1)} all-to-all(bf16[64,6,512]{2,1,0:T(8,128)(2,1)S(1)} %reshape.701), channel_id=1, replica_groups=mesh['sp_0'=8,'sp_1'=4,'sp_2'=2,'tp'=4] {'sp_0','sp_1','sp_2'}, dimensions={0} | all-to-all | bytes 786432 | tf_op jit(solution)/shard_map/all_to_all | solution.py:126
  45.9 1.3 stack.3
  47.2 4.8 all-to-all-start.1
  52.0 2.1 fusion.5
  54.2 1.9 fusion.7
  56.1 14.3 %all-to-all-done.1 = bf16[4,1,384,512]{2,3,1,0:T(8,128)(2,1)} async-done(((bf16[4,1,384,512]{2,3,1,0:T(8,128)(2,1)}), bf16[4,1,384,512]{2,3,1,0:T(8,128)(2,1)}, u32[]{:S(2)}, u32[]{:S(2)}) %all-to-all-start.1) | async-done | bytes 1572896 | tf_op jit(solution)/shard_map/all_to_all | solution.py:139
  70.4 2.3 multiply_convert_fusion.3
  74.2 2.2 add_bitcast_fusion
  77.0 35.6 %reduce-scatter.3.cloned.1.call-done = f32[1,384,512]{2,1,0:T(8,128)} async-done(((f32[1,384,2048]{2,1,0:T(8,128)}), f32[1,384,512]{2,1,0:T(8,128)}) %reduce-scatter.3.cloned.1.call-update) | async-done | bytes 786448 | tf_op jit(solution)/shard_map/reduce_scatter | solution.py:166
  112.7 1.2 convert_element_type.85
  113.9 0.9 reshape_transpose_reshape.3
  114.8 10.5 %all-to-all-start.2 = ((bf16[64,6,512]{2,1,0:T(8,128)(2,1)}), bf16[64,6,512]{2,1,0:T(8,128)(2,1)S(1)}, u32[]{:S(2)}, u32[]{:S(2)}) async-start(bf16[64,6,512]{2,1,0:T(8,128)(2,1)} %reshape_transpose_reshape.3), calls=%async_computation.3 | async-start | bytes 1048576 | tf_op jit(solution)/shard_map/all_to_all | solution.py:171
  125.7 21.9 %all-to-all-done.2 = bf16[64,6,512]{2,1,0:T(8,128)(2,1)S(1)} async-done(((bf16[64,6,512]{2,1,0:T(8,128)(2,1)}), bf16[64,6,512]{2,1,0:T(8,128)(2,1)S(1)}, u32[]{:S(2)}, u32[]{:S(2)}) %all-to-all-start.2) | async-done | bytes 393248 | tf_op jit(solution)/shard_map/all_to_all | solution.py:171
  147.8 1.2 gather_fusion
  149.9 1.7 fusion.97
  151.6 12.0 %all_gather.52 = bf16[128,2048]{1,0:T(8,128)(2,1)S(1)} all-gather(bf16[128,512]{1,0:T(8,128)(2,1)S(1)} %get-tuple-element.222), channel_id=1, replica_groups=mesh['sp_0'=8,'sp_1'=4,'sp_2'=2,'tp'=4] {'tp'}, dimensions={1}, use_global_device_ids=true | all-gather | bytes 655360 | tf_op jit(solution)/shard_map/all_gather | solution.py:179
  163.6 4.0 fusion.70
  167.8 1.2 fusion.60
  169.5 1.8 all-gather
  171.9 10.3 %all-gather.1 = f32[4,1,16]{2,1,0:T(1,128)S(1)} all-gather(f32[1,1,16]{2,1,0:T(1,128)S(1)} %get-tuple-element.301), channel_id=1, replica_groups=mesh['sp_0'=8,'sp_1'=4,'sp_2'=2,'tp'=4] {'sp_1'}, dimensions={0}, use_global_device_ids=true | all-gather | bytes 320 | tf_op jit(solution)/shard_map/all_gather | solution.py:24
  182.9 2.3 multiply_add_fusion.1
  185.8 32.2 %all-gather.25.cloned.1.call-done = f32[4,16,64,128]{3,2,1,0:T(8,128)} async-done(((f32[1,16,64,128]{3,2,1,0:T(8,128)}), f32[4,16,64,128]{3,2,1,0:T(8,128)}) %all-gather.25.cloned.1.call-update) | async-done | bytes 2097168 | tf_op jit(solution)/shard_map/all_gather | solution.py:24
  218.0 3.3 multiply_add_fusion
  223.2 16.8 %all-gather.3 = f32[8,1,16]{2,1,0:T(1,128)S(1)} all-gather(f32[1,1,16]{2,1,0:T(1,128)S(1)} %get-tuple-element.282), channel_id=1, replica_groups=mesh['sp_0'=8,'sp_1'=4,'sp_2'=2,'tp'=4] {'sp_0'}, dimensions={0}, use_global_device_ids=true | all-gather | bytes 576 | tf_op jit(solution)/shard_map/all_gather | solution.py:24
  246.6 29.7 %all-gather.27.cloned.1.call-done = f32[8,16,64,128]{3,2,1,0:T(8,128)} async-done(((f32[1,16,64,128]{3,2,1,0:T(8,128)}), f32[8,16,64,128]{3,2,1,0:T(8,128)}) %all-gather.27.cloned.1.call-update) | async-done | bytes 4194320 | tf_op jit(solution)/shard_map/all_gather | solution.py:24
  276.4 2.6 fusion.100
  279.3 2.6 add_add_fusion
  281.9 1.2 fusion.25
  283.8 1.2 fusion.24
  285.1 12.9 %all-gather.15.cloned.1.call-done = f32[2,16,64,128]{3,2,1,0:T(8,128)} async-done(((f32[1,16,64,128]{3,2,1,0:T(8,128)}), f32[2,16,64,128]{3,2,1,0:T(8,128)}) %all-gather.15.cloned.1.call-update) | async-done | bytes 1048592 | tf_op jit(solution)/shard_map/all_gather | solution.py:24
  298.0 2.4 multiply_add_fusion.3
  300.6 34.7 %all-gather.17.cloned.1.call-done = f32[4,16,64,128]{3,2,1,0:T(8,128)} async-done(((f32[1,16,64,128]{3,2,1,0:T(8,128)}), f32[4,16,64,128]{3,2,1,0:T(8,128)}) %all-gather.17.cloned.1.call-update) | async-done | bytes 2097168 | tf_op jit(solution)/shard_map/all_gather | solution.py:24
  335.3 3.2 multiply_add_fusion.2
  338.9 16.7 %all-gather.2 = f32[8,1,16]{2,1,0:T(1,128)S(1)} all-gather(f32[1,1,16]{2,1,0:T(1,128)S(1)} %copy-done.87), channel_id=1, replica_groups=mesh['sp_0'=8,'sp_1'=4,'sp_2'=2,'tp'=4] {'sp_0'}, dimensions={0}, use_global_device_ids=true | all-gather | bytes 576 | tf_op jit(solution)/shard_map/all_gather | solution.py:24
  361.7 0.8 copy.88
  363.1 30.4 %all-gather.19.cloned.1.call-done = f32[8,16,64,128]{3,2,1,0:T(8,128)} async-done(((f32[1,16,64,128]{3,2,1,0:T(8,128)}), f32[8,16,64,128]{3,2,1,0:T(8,128)}) %all-gather.19.cloned.1.call-update) | async-done | bytes 4194320 | tf_op jit(solution)/shard_map/all_gather | solution.py:24
  393.6 2.6 fusion.99
  396.7 1.4 add_add_fusion.1
  398.1 1.0 multiply_reduce_fusion.1
  399.1 2.1 fusion.10
  401.3 1.2 copy.94
  402.5 5.9 %fusion.64 = f32[2048,1024]{1,0:T(8,128)} fusion(bf16[128,2048]{1,0:T(8,128)(2,1)} %copy-done.7, f32[128,1024]{1,0:T(8,128)S(1)} %copy.94, bf16[128,1024]{1,0:T(8,128)(2,1)} %param.25), kind=kOutput, calls=%fused_computation.127 | convolution fusion | flops 537788416 | bytes 9699328 | tf_op jit(solution)/shard_map/dot_general | solution.py:234
  409.7 1.7 fusion
  411.4 2.3 copy.107
  413.7 1.7 fusion.1
  415.4 2.3 copy.108
  417.7 3.2 fusion.2
  420.9 1.5 fusion.23
  422.6 0.7 copy.104
  423.9 1.0 convolution_bitcast_fusion.6
  425.2 0.8 copy.110
  425.9 3.3 fusion.9
  429.3 2.1 copy.109
  431.4 1.0 convolution_bitcast_fusion.5
  432.7 0.8 copy.111
  433.5 0.7 copy.103
  434.3 6.7 %fusion.36 = f32[16]{0:T(128)S(1)} fusion(f32[16]{0:T(128)} %copy-done.69, f32[16]{0:T(128)S(1)} %copy-done.65, f32[16]{0:T(128)} %copy-done.66, f32[16]{0:T(128)} %copy-done.71, f32[16]{0:T(128)} %get-tuple-element.215, f32[16]{0:T(128)} %get-tuple-element.278, f32[16]{0:T(128)} %get-tuple-element.277, f32[16]{0:T(128)} %get-tuple-element.276, ...), kind=kLoop, calls=%fused_computation.59 | loop fusion | flops 11534320 | bytes 14682076 | tf_op jit(solution)/shard_map/transpose(jvp())/while/body/eval_jaxpr/reduce_sum | solution.py:61
  441.2 1.1 reduce_window_sum.44
  443.0 2.2 fusion.31
  445.2 114.5 %reduce-scatter.5.cloned.1.call-done = f32[32,1024]{1,0:T(8,128)} async-done(((f32[2048,1024]{1,0:T(8,128)}), f32[32,1024]{1,0:T(8,128)}) %reduce-scatter.5.cloned.1.call-update) | async-done | bytes 131088 | tf_op jit(solution)/shard_map/reduce_scatter | solution.py:233
  (323 shorter events, 30.2 us)
Async XLA Ops:
  8.0 44.0 %copy-start = (bf16[1,2048,256]{2,1,0:T(8,128)(2,1)S(1)}, bf16[1,2048,256]{2,1,0:T(8,128)(2,1)}, u32[]{:S(2)}) copy-start(bf16[1,2048,256]{2,1,0:T(8,128)(2,1)} %param.17) | copy-start | bytes 3145732
  8.0 44.0 %all-gather.13.cloned.1.call-start = ((), (), s32[]{:S(2)}) async-start(), calls=%async_computation.5 | async-start | bytes 1966080 | tf_op jit(solution)/shard_map/all_gather | solution.py:141
  47.2 23.2 %all-to-all-start.1 = ((bf16[4,1,384,512]{2,3,1,0:T(8,128)(2,1)}), bf16[4,1,384,512]{2,3,1,0:T(8,128)(2,1)}, u32[]{:S(2)}, u32[]{:S(2)}) async-start(bf16[4,1,384,512]{2,3,1,0:T(8,128)(2,1)} %stack.3), calls=%async_computation.1 | async-start | bytes 3145728 | tf_op jit(solution)/shard_map/all_to_all | solution.py:139
  52.0 60.7 %reduce-scatter.3.cloned.1.call-start = ((), (), s32[]{:S(2)}) async-start(), calls=%async_computation.6 | async-start | bytes 3932160 | tf_op jit(solution)/shard_map/reduce_scatter | solution.py:166
  54.1 18.6 %copy-start.107 = (f32[384,256]{1,0:T(8,128)}, f32[384,256]{1,0:T(8,128)S(1)}, u32[]{:S(2)}) copy-start(f32[384,256]{1,0:T(8,128)S(1)} %fusion.5) | copy-start | bytes 1179652
  56.1 16.7 %copy-start.109 = (f32[384,256]{1,0:T(8,128)}, f32[384,256]{1,0:T(8,128)S(1)}, u32[]{:S(2)}) copy-start(f32[384,256]{1,0:T(8,128)S(1)} %fusion.7) | copy-start | bytes 1179652
  76.4 48.9 %copy-start.44 = (bf16[128,256]{1,0:T(8,128)(2,1)S(1)}, bf16[128,256]{1,0:T(8,128)(2,1)}, u32[]{:S(2)}) copy-start(bf16[128,256]{1,0:T(8,128)(2,1)} %param.23) | copy-start | bytes 196612
  76.4 48.9 %copy-start.61 = (f32[128,16]{0,1:T(8,128)S(1)}, f32[128,16]{0,1:T(8,128)}, u32[]{:S(2)}) copy-start(f32[128,16]{0,1:T(8,128)} %param.24) | copy-start | bytes 24580
  76.5 87.1 %all-gather.21.cloned.1.call-start = ((), (), s32[]{:S(2)}) async-start(), calls=%async_computation.11 | async-start | bytes 4259840 | tf_op jit(solution)/shard_map/all_gather | solution.py:208
  114.8 32.9 %all-to-all-start.2 = ((bf16[64,6,512]{2,1,0:T(8,128)(2,1)}), bf16[64,6,512]{2,1,0:T(8,128)(2,1)S(1)}, u32[]{:S(2)}, u32[]{:S(2)}) async-start(bf16[64,6,512]{2,1,0:T(8,128)(2,1)} %reshape_transpose_reshape.3), calls=%async_computation.3 | async-start | bytes 1048576 | tf_op jit(solution)/shard_map/all_to_all | solution.py:171
  125.3 57.6 %all-gather.23.cloned.1.call-start = ((), (), s32[]{:S(2)}) async-start(), calls=%async_computation.12 | async-start | bytes 1572864 | tf_op jit(solution)/shard_map/all_gather | solution.py:24
  125.6 43.4 %copy-start.26 = (f32[128,16]{1,0:T(8,128)}, f32[128,16]{1,0:T(8,128)S(1)}, u32[]{:S(2)}) copy-start(f32[128,16]{1,0:T(8,128)S(1)} %reduce_window_sum.43) | copy-start | bytes 24580
  125.7 42.0 %copy-start.37 = (f32[128,2,8]{0,2,1:T(8,128)}, f32[128,2,8]{0,2,1:T(8,128)S(1)}, u32[]{:S(2)}) copy-start(f32[128,2,8]{0,2,1:T(8,128)S(1)} %bitcast_exponential_fusion) | copy-start | bytes 24580
  149.0 14.6 %copy-start.19 = (bf16[128,1024]{1,0:T(8,128)(2,1)S(1)}, bf16[128,1024]{1,0:T(8,128)(2,1)}, u32[]{:S(2)}) copy-start(bf16[128,1024]{1,0:T(8,128)(2,1)} %param.25) | copy-start | bytes 786436
  163.6 4.0 copy-start.7
  168.9 49.1 %all-gather.25.cloned.1.call-start = ((), (), s32[]{:S(2)}) async-start(), calls=%async_computation.13 | async-start | bytes 2621440 | tf_op jit(solution)/shard_map/all_gather | solution.py:24
  171.3 49.9 %copy-start.53 = (f32[2,1,16]{2,1,0:T(1,128)}, f32[2,1,16]{2,1,0:T(1,128)S(1)}, u32[]{:S(2)}) copy-start(f32[2,1,16]{2,1,0:T(1,128)S(1)} %all-gather) | copy-start | bytes 388
  171.9 13.2 %copy-start.64 = (f32[16]{0:T(128)}, f32[16]{0:T(128)S(1)}, u32[]{:S(2)}) copy-start(f32[16]{0:T(128)S(1)} %get-tuple-element.298) | copy-start | bytes 196
  182.2 40.4 %copy-start.46 = (f32[4,1,16]{2,1,0:T(1,128)}, f32[4,1,16]{2,1,0:T(1,128)S(1)}, u32[]{:S(2)}) copy-start(f32[4,1,16]{2,1,0:T(1,128)S(1)} %all-gather.1) | copy-start | bytes 772
  182.8 38.4 %copy-start.66 = (f32[16]{0:T(128)}, f32[16]{0:T(128)S(1)}, u32[]{:S(2)}) copy-start(f32[16]{0:T(128)S(1)} %get-tuple-element.279) | copy-start | bytes 196
  185.2 91.1 %all-gather.27.cloned.1.call-start = ((), (), s32[]{:S(2)}) async-start(), calls=%async_computation.14 | async-start | bytes 4718592 | tf_op jit(solution)/shard_map/all_gather | solution.py:24
  185.8 35.5 %copy-start.55 = (f32[16]{0:T(128)}, f32[16]{0:T(128)S(1)}, u32[]{:S(2)}) copy-start(f32[16]{0:T(128)S(1)} %get-tuple-element.284) | copy-start | bytes 196
  185.8 35.5 %copy-start.58 = (f32[16]{0:T(128)}, f32[16]{0:T(128)S(1)}, u32[]{:S(2)}) copy-start(f32[16]{0:T(128)S(1)} %get-tuple-element.286) | copy-start | bytes 196
  185.8 35.5 %copy-start.71 = (f32[16]{0:T(128)}, f32[16]{0:T(128)S(1)}, u32[]{:S(2)}) copy-start(f32[16]{0:T(128)S(1)} %get-tuple-element.285) | copy-start | bytes 196
  218.0 27.8 %copy-start.34 = (bf16[128,1024]{1,0:T(8,128)(2,1)S(1)}, bf16[128,1024]{1,0:T(8,128)(2,1)}, u32[]{:S(2)}) copy-start(bf16[128,1024]{1,0:T(8,128)(2,1)} %param.21) | copy-start | bytes 786436
  221.3 76.7 %all-gather.15.cloned.1.call-start = ((), (), s32[]{:S(2)}) async-start(), calls=%async_computation.7 | async-start | bytes 1572864 | tf_op jit(solution)/shard_map/all_gather | solution.py:24
  222.2 56.8 %copy-start.80 = (f32[2,8]{1,0:T(2,128)}, f32[2,8]{1,0:T(2,128)S(1)}, u32[]{:S(2)}) copy-start(f32[2,8]{1,0:T(2,128)S(1)} %squeeze.234) | copy-start | bytes 196
  222.3 56.7 %copy-start.72 = (f32[2,8]{1,0:T(2,128)}, f32[2,8]{1,0:T(2,128)S(1)}, u32[]{:S(2)}) copy-start(f32[2,8]{1,0:T(2,128)S(1)} %squeeze.235) | copy-start | bytes 196
  222.4 56.7 %copy-start.81 = (f32[2,8]{1,0:T(2,128)}, f32[2,8]{1,0:T(2,128)S(1)}, u32[]{:S(2)}) copy-start(f32[2,8]{1,0:T(2,128)S(1)} %squeeze.230) | copy-start | bytes 196
  222.4 56.6 %copy-start.49 = (f32[2,8]{1,0:T(2,128)}, f32[2,8]{1,0:T(2,128)S(1)}, u32[]{:S(2)}) copy-start(f32[2,8]{1,0:T(2,128)S(1)} %squeeze.231) | copy-start | bytes 196
  222.5 56.5 %copy-start.51 = (f32[2,8]{1,0:T(2,128)}, f32[2,8]{1,0:T(2,128)S(1)}, u32[]{:S(2)}) copy-start(f32[2,8]{1,0:T(2,128)S(1)} %squeeze.232) | copy-start | bytes 196
  222.6 56.4 %copy-start.74 = (f32[2,8]{1,0:T(2,128)}, f32[2,8]{1,0:T(2,128)S(1)}, u32[]{:S(2)}) copy-start(f32[2,8]{1,0:T(2,128)S(1)} %squeeze.233) | copy-start | bytes 196
  279.3 3.9 copy-start.105
  281.9 16.1 %copy-start.62 = (f32[16]{0:T(128)S(1)}, f32[16]{0:T(128)}, u32[]{:S(2)}) copy-start(f32[16]{0:T(128)} %get-tuple-element.297) | copy-start | bytes 196
  281.9 16.1 %copy-start.68 = (f32[16]{0:T(128)S(1)}, f32[16]{0:T(128)}, u32[]{:S(2)}) copy-start(f32[16]{0:T(128)} %get-tuple-element.291) | copy-start | bytes 196
  283.1 17.4 %copy-start.40 = (f32[128,2,8]{0,2,1:T(8,128)}, f32[128,2,8]{0,2,1:T(8,128)S(1)}, u32[]{:S(2)}) copy-start(f32[128,2,8]{0,2,1:T(8,128)S(1)} %get-tuple-element.304) | copy-start | bytes 24580
  283.8 51.5 %copy-start.56 = (f32[16]{0:T(128)S(1)}, f32[16]{0:T(128)}, u32[]{:S(2)}) copy-start(f32[16]{0:T(128)} %copy-done.55) | copy-start | bytes 196
  283.8 51.5 %copy-start.59 = (f32[16]{0:T(128)S(1)}, f32[16]{0:T(128)}, u32[]{:S(2)}) copy-start(f32[16]{0:T(128)} %copy-done.58) | copy-start | bytes 196
  283.8 51.5 %copy-start.67 = (f32[16]{0:T(128)S(1)}, f32[16]{0:T(128)}, u32[]{:S(2)}) copy-start(f32[16]{0:T(128)} %get-tuple-element.280) | copy-start | bytes 196
  283.8 51.5 %copy-start.70 = (f32[16]{0:T(128)S(1)}, f32[16]{0:T(128)}, u32[]{:S(2)}) copy-start(f32[16]{0:T(128)} %get-tuple-element.283) | copy-start | bytes 196
  285.1 50.2 %all-gather.17.cloned.1.call-start = ((), (), s32[]{:S(2)}) async-start(), calls=%async_computation.8 | async-start | bytes 2621440 | tf_op jit(solution)/shard_map/all_gather | solution.py:24
  300.5 92.9 %all-gather.19.cloned.1.call-start = ((), (), s32[]{:S(2)}) async-start(), calls=%async_computation.9 | async-start | bytes 4718592 | tf_op jit(solution)/shard_map/all_gather | solution.py:24
  338.6 221.2 %reduce-scatter.5.cloned.1.call-start = ((), (), s32[]{:S(2)}) async-start(), calls=%async_computation.10 | async-start | bytes 8519680 | tf_op jit(solution)/shard_map/reduce_scatter | solution.py:233
  338.8 57.5 %copy-start.28 = (bf16[128,2,128]{0,2,1:T(8,128)(2,1)}, bf16[128,2,128]{0,2,1:T(8,128)(2,1)S(1)}, u32[]{:S(2)}) copy-start(bf16[128,2,128]{0,2,1:T(8,128)(2,1)S(1)} %copy.101) | copy-start | bytes 196612
  402.5 5.9 %copy-start.4 = (f32[128,1024]{1,0:T(8,128)}, f32[128,1024]{1,0:T(8,128)S(1)}, u32[]{:S(2)}) copy-start(f32[128,1024]{1,0:T(8,128)S(1)} %copy.94) | copy-start | bytes 1572868
  409.7 4.0 copy-start.25
  423.9 7.5 %copy-start.6 = (f32[2,8,64,128]{3,2,1,0:T(8,128)S(1)}, f32[2,8,64,128]{3,2,1,0:T(8,128)}, u32[]{:S(2)}) copy-start(f32[2,8,64,128]{3,2,1,0:T(8,128)} %copy-done.5) | copy-start | bytes 1572868
  424.9 6.4 %copy-start.41 = (f32[128,2,8]{0,2,1:T(8,128)S(1)}, f32[128,2,8]{0,2,1:T(8,128)}, u32[]{:S(2)}) copy-start(f32[128,2,8]{0,2,1:T(8,128)} %copy-done.40) | copy-start | bytes 24580
  424.9 6.5 %copy-start.39 = (f32[128,2,8]{0,2,1:T(8,128)S(1)}, f32[128,2,8]{0,2,1:T(8,128)}, u32[]{:S(2)}) copy-start(f32[128,2,8]{0,2,1:T(8,128)} %copy-done.37) | copy-start | bytes 24580
  425.1 7.3 %copy-start.29 = (bf16[128,2,128]{0,2,1:T(8,128)(2,1)S(1)}, bf16[128,2,128]{0,2,1:T(8,128)(2,1)}, u32[]{:S(2)}) copy-start(bf16[128,2,128]{0,2,1:T(8,128)(2,1)} %copy-done.28) | copy-start | bytes 196612
  425.9 6.6 %copy-start.31 = (f32[128,128,2]{1,0,2:T(8,128)S(1)}, f32[128,128,2]{1,0,2:T(8,128)}, u32[]{:S(2)}) copy-start(f32[128,128,2]{1,0,2:T(8,128)} %copy-done.30) | copy-start | bytes 393220
  425.9 7.6 %copy-start.48 = (f32[128,2,8]{0,2,1:T(8,128)S(1)}, f32[128,2,8]{0,2,1:T(8,128)}, u32[]{:S(2)}) copy-start(f32[128,2,8]{0,2,1:T(8,128)} %get-tuple-element.306) | copy-start | bytes 24580
  425.9 8.3 %copy-start.2 = (f32[4,16,64,128]{3,2,1,0:T(8,128)S(1)}, f32[4,16,64,128]{3,2,1,0:T(8,128)}, u32[]{:S(2)}) copy-start(f32[4,16,64,128]{3,2,1,0:T(8,128)} %all-gather.25.cloned.1.call-done) | copy-start | bytes 6291460
  429.3 5.0 copy-start.57
  429.3 5.0 copy-start.60
  429.3 5.0 copy-start.63
  429.3 5.0 copy-start.65
  434.3 6.8 %copy-start.27 = (f32[128,16]{1,0:T(8,128)S(1)}, f32[128,16]{1,0:T(8,128)}, u32[]{:S(2)}) copy-start(f32[128,16]{1,0:T(8,128)} %copy-done.26) | copy-start | bytes 24580
  434.3 6.8 %copy-start.35 = (f32[128,16]{1,0:T(8,128)S(1)}, f32[128,16]{1,0:T(8,128)}, u32[]{:S(2)}) copy-start(f32[128,16]{1,0:T(8,128)} %copy.104) | copy-start | bytes 24580
  434.3 6.8 %copy-start.36 = (f32[128,16]{1,0:T(8,128)S(1)}, f32[128,16]{1,0:T(8,128)}, u32[]{:S(2)}) copy-start(f32[128,16]{1,0:T(8,128)} %copy.103) | copy-start | bytes 24580
  434.3 6.8 %copy-start.86 = (f32[16]{0:T(128)S(1)}, f32[16]{0:T(128)}, u32[]{:S(2)}) copy-start(f32[16]{0:T(128)} %get-tuple-element.258) | copy-start | bytes 196
  434.3 6.8 %copy-start.106 = (f32[1,16]{1,0:T(1,128)S(1)}, f32[1,16]{1,0:T(1,128)}, u32[]{:S(2)}) copy-start(f32[1,16]{1,0:T(1,128)} %reshape.717) | copy-start | bytes 196
  434.3 8.7 %copy-start.20 = (bf16[128,1024]{1,0:T(8,128)(2,1)S(1)}, bf16[128,1024]{1,0:T(8,128)(2,1)}, u32[]{:S(2)}) copy-start(bf16[128,1024]{1,0:T(8,128)(2,1)} %param.25) | copy-start | bytes 786436
  434.3 125.4 %copy-start.1 = (bf16[1,2048,256]{2,1,0:T(8,128)(2,1)S(1)}, bf16[1,2048,256]{2,1,0:T(8,128)(2,1)}, u32[]{:S(2)}) copy-start(bf16[1,2048,256]{2,1,0:T(8,128)(2,1)} %param.17) | copy-start | bytes 3145732
  (59 other events, 159.4 us)
Sparse Core Ops, SparseCore 0:
  10.6 30.5 all-gather.12
  76.5 36.0 reduce-scatter.2
  185.3 32.6 all-gather.24
  300.6 34.6 all-gather.16
Sparse Core Ops, SparseCore 1:
  79.7 79.4 all-gather.20
  169.0 11.8 all-gather.22
  221.4 54.8 all-gather.26
  285.1 12.8 all-gather.14
  338.6 54.7 all-gather.18
  408.5 151.1 reduce-scatter.4
